TPU v7x, 32 devices: a whole 2x2x4 slice. The times are simulated.
32 devices in a mesh: ep: 8 (over z, x), tp: 4 (over y, core).
Axes of the slice: x: 2, y: 2, z: 4, core: 2. Of those that a mesh axis runs over, the one named last changes fastest.
Arguments:
- recurrence_query: bfloat16 [1024, 1024], P('ep', 'tp'), may hold values from -6 to 6
- forget_preactivation: bfloat16 [1024, 1024], P('ep', 'tp'), may hold values from -7 to 7
- recurrence_value: bfloat16 [1024, 1024], P('ep', 'tp'), may hold values from -6 to 6
- output_gate_preactivation: bfloat16 [1024, 1024], P('ep', 'tp'), may hold values from -6 to 6
- forget_margin: float32 [1024], P('tp'), may hold values from 0 to 0.1
- surge_log_decay: float32 [8, 1024], P('tp', 'ep'), may hold values from -1.4 to 0
- head_norm_gain: float32 [1024], P('tp'), may hold values from 0.1 to 1.9
- recurrence_output_matrix: bfloat16 [1024, 4096], P('tp'), may hold values from -0.1875 to 0.1875
- second_micro_input: bfloat16 [1024, 4096], P(('ep', 'tp')), may hold values from -6 to 6
- expert_norm_gain: float32 [4096], replicated, may hold values from 0.1 to 1.9
- routes: int32 [1024, 2], P('ep'), may hold values from 0 to 7, all different within a row; in each aligned block of 32 rows (0 to 31, 32 to 63, ...) at most 16 rows name the same one
- router_chosen_logits: float32 [1024, 2], P(('ep', 'tp')), may hold values from -6 to 6
- expert_gate_matrix: bfloat16 [8, 4096, 1408], P('ep', None, 'tp'), may hold values from -0.09375 to 0.09375
- expert_up_matrix: bfloat16 [8, 4096, 1408], P('ep', None, 'tp'), may hold values from -0.09375 to 0.09375
- expert_down_matrix: bfloat16 [8, 1408, 4096], P('ep', 'tp'), may hold values from -0.15625 to 0.15625
Outputs:
- mixed: bfloat16 [1024, 4096], P(('ep', 'tp'))
- moe_out: bfloat16 [1024, 4096], P(('ep', 'tp'))
Inputs may be any that keep to these rules, and one draw needn't show every extreme that they name: `routes`: in the rows of one device (aligned blocks of 32 rows) no expert is named more than 16 times, and the experts of a row differ.
All inputs are finite; a program needn't handle non-finite values.
Results may differ from a plain program's by a relative error of at most 0.019.
Values may be sent and summed in bfloat16 or wider, within the bound.
A program may use at most 128 MiB of HBM per device.

v0:
```python
import functools

import jax
import jax.numpy as jnp
from jax import lax
from jax.experimental import pallas as pl
from jax.experimental.pallas import tpu as pltpu
from jax.sharding import PartitionSpec as P

TOP = 2
SPAN = 64
MESH = pl.DeviceIdType.MESH


epsilon = 1e-06
highest = lax.Precision.HIGHEST


def visiting_order(count):
    return sorted(range(1, count), key=lambda k: abs(k - count // 2)) + [0]


def greet(me, tp, ep_count, tp_count, wait=True):
    pairs = tp_count // 2
    pair, side = tp // 2, tp % 2
    barrier = pltpu.get_barrier_semaphore()
    for k in range(1, ep_count):
        pl.semaphore_signal(
            barrier,
            inc=1,
            device_id={"ep": lax.rem(me + k, ep_count), "tp": tp},
            device_id_type=MESH,
        )
    for j in range(1, pairs):
        pl.semaphore_signal(
            barrier,
            inc=1,
            device_id={"ep": me, "tp": lax.rem(pair + j, pairs) * 2 + side},
            device_id_type=MESH,
        )
    pl.semaphore_signal(
        barrier, inc=1, device_id={"ep": me, "tp": pair * 2 + 1 - side}, device_id_type=MESH
    )
    if wait:
        pl.semaphore_wait(barrier, ep_count + pairs - 1)


def product(left, right, left_axis, right_axis, precision=None):
    return lax.dot_general(
        left,
        right,
        (((left_axis,), (right_axis,)), ((), ())),
        precision=precision,
        preferred_element_type=jnp.float32,
    )


def iota(shape, axis):
    return lax.broadcasted_iota(jnp.int32, shape, axis)


def dispatch_kernel(
    ep_count,
    tp_count,
    query_ref,
    forget_ref,
    value_ref,
    opening_ref,
    margin_ref,
    surge_ref,
    head_gain_ref,
    tokens_ref,
    gain_ref,
    routes_ref,
    logits_ref,
    gate_hbm,
    up_hbm,
    hidden_b_ref,
    hidden_a_ref,
    weights_ref,
    slots,
    piece,
    gate,
    up,
    lifted_ref,
    local_ref,
    window,
    window_total,
    before,
    before_total,
    outgoing,
    incoming,
    load,
    sa,
    ra,
    sy,
    ry,
    sc,
    rc,
    ss,
    rs,
):
    wide = jnp.float32
    me, tp = lax.axis_index("ep"), lax.axis_index("tp")
    pairs = tp_count // 2
    pair, side = tp // 2, tp % 2
    other = pair * 2 + 1 - side
    order = visiting_order(ep_count)
    heads, seq_len = surge_ref.shape
    key_width = query_ref.shape[1] // heads
    value_width = value_ref.shape[1] // heads
    tok_rows = tokens_ref.shape[0]
    capacity = slots.shape[1]
    slot_count = ep_count * capacity
    steps = outgoing.shape[0]

    greet(me, tp, ep_count, tp_count, wait=False)
    fetch = [
        pltpu.make_async_copy(gate_hbm, gate, load.at[0]),
        pltpu.make_async_copy(up_hbm, up, load.at[1]),
    ]
    for copy in fetch:
        copy.start()

    def remote(src, dst, send, recv, ep, to):
        return pltpu.make_async_remote_copy(
            src_ref=src,
            dst_ref=dst,
            send_sem=send,
            recv_sem=recv,
            device_id={"ep": ep, "tp": to},
            device_id_type=MESH,
        )

    def exchange(k):
        to = lax.rem(me + k, ep_count)
        return remote(slots.at[to], piece.at[tp, me], sa.at[k], ra.at[k], to, tp)

    def source(k):
        return lax.rem(me + ep_count - k, ep_count)

    def own_block(k):
        return slots.at[me] if k == 0 else piece.at[tp, source(k)]

    def across(k, j):
        to = lax.rem(pair + j, pairs) * 2 + side
        return remote(own_block(k), piece.at[tp, source(k)], sy.at[j, k], ry.at[j, k], me, to)

    def beside(k, j):
        block = lax.rem(pair + pairs - j, pairs) * 2 + side
        src = own_block(k) if j == 0 else piece.at[block, source(k)]
        return remote(src, piece.at[block, source(k)], sc.at[j, k], rc.at[j, k], me, other)

    def pass_on(k):
        for j in range(1, pairs):
            across(k, j).start()
        beside(k, 0).start()

    rows = tokens_ref[...].astype(wide)
    normed = (
        rows * lax.rsqrt(jnp.mean(rows * rows, axis=-1, keepdims=True) + epsilon) * gain_ref[...]
    ).astype(jnp.bfloat16)
    routes = routes_ref[pl.ds(pl.multiple_of(tp * tok_rows, tok_rows), tok_rows), :]
    named = [routes[:, i : i + 1] for i in range(TOP)]
    experts = iota((tok_rows, ep_count), 1)
    tables = [(column == experts).astype(wide) for column in named]
    strict = (iota((tok_rows, tok_rows), 0) > iota((tok_rows, tok_rows), 1)).astype(wide)
    earlier = product(strict, sum(tables), 1, 0, highest)
    places = [jnp.sum(earlier * table, axis=1, keepdims=True) for table in tables]
    spots = [
        column * capacity + place.astype(jnp.int32) for column, place in zip(named, places)
    ]
    for number, k in enumerate(order):
        to = lax.rem(me + k, ep_count)
        wanted = iota((tok_rows, capacity), 1) + to * capacity
        chooser = sum((spot == wanted).astype(wide) for spot in spots).astype(jnp.bfloat16)
        slots[to] = product(chooser, normed, 0, 0).astype(jnp.bfloat16)
        if number == 0:
            pl.semaphore_wait(pltpu.get_barrier_semaphore(), ep_count + pairs - 1)
        if k:
            exchange(k).start()
    pass_on(0)
    piece[tp, me] = slots[me]

    at, since = iota((seq_len, seq_len), 0), iota((seq_len, seq_len), 1)
    shut = jax.nn.sigmoid(-forget_ref[...].astype(wide)) * margin_ref[...]
    logarithm = jnp.log1p(-shut)
    within = ((at >= since) & (at // SPAN == since // SPAN)).astype(wide)
    running_all = product(within, logarithm, 1, 0, highest)
    triangle = iota((SPAN, SPAN), 0) >= iota((SPAN, SPAN), 1)
    for head in range(heads):
        keys = slice(head * key_width, (head + 1) * key_width)
        values = slice(head * value_width, (head + 1) * value_width)
        surges = jnp.sum(within * surge_ref[head : head + 1, :], axis=1, keepdims=True)
        running_head = running_all[:, keys] + surges
        state = jnp.zeros((value_width, key_width), wide)
        total = jnp.zeros((1, key_width), wide)
        for span in range(seq_len // SPAN):
            part = slice(span * SPAN, (span + 1) * SPAN)
            running = running_head[part]
            closing = running[SPAN - 1 : SPAN]
            inflow = shut[part, keys]
            value = value_ref[part, values].astype(wide)
            query = query_ref[part, keys].astype(wide)
            lifted = query * jnp.exp(running)
            scores = product(lifted, inflow * jnp.exp(-running), 1, 1, highest)
            scores = jnp.where(triangle, scores, 0.0)
            local = product(scores, value, 1, 0, highest)
            if span:
                local = local + product(lifted, state, 1, 1, highest)
            local_ref[part, values] = local
            lifted_ref[part, keys] = query * jnp.exp(running + total)
            fresh = product(value, inflow * jnp.exp(closing - running), 0, 0, highest)
            state = jnp.exp(closing) * state + fresh
            total = total + closing
        window[head] = state
        window_total[head] = total
    before[...] = jnp.zeros_like(before)
    before_total[...] = jnp.zeros_like(before_total)

    def state_copy(step):
        to = lax.rem(me + 2**step, ep_count)
        return remote(outgoing.at[step], incoming.at[step], ss.at[step], rs.at[step], to, tp)

    def send_window(step):
        for head in range(heads):
            outgoing[step, head, :value_width] = window[head].astype(jnp.bfloat16)
            total = window_total[head]
            coarse = total.astype(jnp.bfloat16).astype(wide)
            line = iota((16, key_width), 0)
            tail = jnp.where(line == 0, coarse, jnp.where(line == 1, total - coarse, 0.0))
            outgoing[step, head, value_width:] = tail.astype(jnp.bfloat16)

        @pl.when(me + 2**step < ep_count)
        def _():
            state_copy(step).start()

    def take_window(step):
        @pl.when(me >= 2**step)
        def _():
            state_copy(step).wait_recv()
            for head in range(heads):
                state = incoming[step, head, :value_width].astype(wide)
                total = jnp.sum(
                    incoming[step, head, value_width:].astype(wide), axis=0, keepdims=True
                )
                before[head] = jnp.exp(before_total[head]) * state + before[head]
                before_total[head] = before_total[head] + total
                window[head] = jnp.exp(window_total[head]) * state + window[head]
                window_total[head] = window_total[head] + total

    sequence = [0] + order[:-1]
    done = 0
    send_window(0)
    for position, k in enumerate(sequence):
        if k:
            exchange(k).wait_recv()
            pass_on(k)
        if position:
            last = sequence[position - 1]
            for j in range(1, pairs):
                across(last, j).wait_recv()
                beside(last, j).start()
        if position >= 2 and position % 2 == 0 and done < steps:
            take_window(done)
            done += 1
            if done < steps:
                send_window(done)
    while done < steps:
        take_window(done)
        done += 1
        if done < steps:
            send_window(done)
    for j in range(1, pairs):
        across(sequence[-1], j).wait_recv()
        beside(sequence[-1], j).start()

    for head in range(heads):
        keys = slice(head * key_width, (head + 1) * key_width)
        values = slice(head * value_width, (head + 1) * value_width)
        out = local_ref[:, values] + product(lifted_ref[:, keys], before[head], 1, 1, highest)
        out = out * lax.rsqrt(jnp.mean(out * out, axis=-1, keepdims=True) + epsilon)
        opening = opening_ref[:, values].astype(wide)
        hidden_a_ref[:, values] = (
            out * head_gain_ref[:, values] * (opening * jax.nn.sigmoid(opening))
        ).astype(jnp.bfloat16)
    logits = logits_ref[...]
    raised = jnp.exp(logits - jnp.max(logits, axis=-1, keepdims=True))
    share = raised / jnp.sum(raised, axis=-1, keepdims=True)
    numbers = iota((tok_rows, slot_count), 1)
    weights_ref[...] = sum(
        jnp.where(spot == numbers, share[:, i : i + 1], 0.0) for i, spot in enumerate(spots)
    )

    for k in sequence:
        for j in range(pairs):
            beside(k, j).wait_recv()
    for copy in fetch:
        copy.wait()

    def experts_of(block, carry):
        if capacity % 16:
            taken = jnp.concatenate([piece[block, e] for e in range(ep_count)], axis=0)
        else:
            taken = piece[block].reshape(slot_count, piece.shape[-1])
        left = product(taken, gate[...], 1, 1)
        right = product(taken, up[...], 1, 1)
        hidden_b_ref[block] = (left * jax.nn.sigmoid(left) * right).astype(jnp.bfloat16)
        return carry

    lax.fori_loop(0, tp_count, experts_of, 0)

    for k in range(1, ep_count):
        exchange(k).wait_send()
    for k in sequence:
        for j in range(pairs):
            if j:
                across(k, j).wait_send()
            beside(k, j).wait_send()
    for step in range(steps):

        @pl.when(me + 2**step < ep_count)
        def _(step=step):
            state_copy(step).wait_send()


def dispatch(small, gate, up, heads, capacity, ep_count, tp_count):
    pairs = tp_count // 2
    dma = pltpu.SemaphoreType.DMA
    vmem = pl.BlockSpec(memory_space=pltpu.VMEM)
    hbm = pl.BlockSpec(memory_space=pl.ANY)
    query, value, tokens = small[0], small[2], small[7]
    seq_len, keys = query.shape
    values = value.shape[1]
    tok_rows, width = tokens.shape
    key_width, value_width = keys // heads, values // heads
    steps = (ep_count - 1).bit_length()
    both = dma((pairs, ep_count))
    kind = jnp.bfloat16
    return pl.pallas_call(
        functools.partial(dispatch_kernel, ep_count, tp_count),
        out_shape=(
            jax.ShapeDtypeStruct((tp_count, ep_count * capacity, gate.shape[0]), kind),
            jax.ShapeDtypeStruct((seq_len, values), kind),
            jax.ShapeDtypeStruct((tok_rows, ep_count * capacity), jnp.float32),
        ),
        in_specs=[vmem] * len(small) + [hbm] * 2,
        out_specs=(vmem, vmem, vmem),
        scratch_shapes=[
            pltpu.VMEM((ep_count, capacity, width), kind),
            pltpu.VMEM((tp_count, ep_count, capacity, width), kind),
            pltpu.VMEM(gate.shape, kind),
            pltpu.VMEM(up.shape, kind),
            pltpu.VMEM((seq_len, keys), jnp.float32),
            pltpu.VMEM((seq_len, values), jnp.float32),
            pltpu.VMEM((heads, value_width, key_width), jnp.float32),
            pltpu.VMEM((heads, 1, key_width), jnp.float32),
            pltpu.VMEM((heads, value_width, key_width), jnp.float32),
            pltpu.VMEM((heads, 1, key_width), jnp.float32),
            pltpu.VMEM((steps, heads, value_width + 16, key_width), kind),
            pltpu.VMEM((steps, heads, value_width + 16, key_width), kind),
            dma((2,)),
            dma((ep_count,)),
            dma((ep_count,)),
            both,
            both,
            both,
            both,
            dma((steps,)),
            dma((steps,)),
        ],
        compiler_params=pltpu.CompilerParams(
            collective_id=0, has_side_effects=True, vmem_limit_bytes=60 << 20
        ),
    )(*small, gate, up)


def return_kernel(
    ep_count,
    tp_count,
    parts,
    mix,
    mixed,
    returned,
    cbuf,
    cmix,
    ysend,
    ysmix,
    ybuf,
    ymix,
    abuf,
    sc,
    rc,
    sy,
    ry,
    sa,
    ra,
):
    me, tp = lax.axis_index("ep"), lax.axis_index("tp")
    pairs = tp_count // 2
    pair, side = tp // 2, tp % 2
    other = pair * 2 + 1 - side
    order = visiting_order(ep_count)
    greet(me, tp, ep_count, tp_count)

    def remote(src, dst, send, recv, ep, to):
        return pltpu.make_async_remote_copy(
            src_ref=src,
            dst_ref=dst,
            send_sem=send,
            recv_sem=recv,
            device_id={"ep": ep, "tp": to},
            device_id_type=MESH,
        )

    def chunk(k):
        return lax.rem(me + k, ep_count)

    def toward(j):
        return lax.rem(pair + j, pairs)

    def beside(k, j):
        block = toward(j) * 2 + 1 - side
        if k == ep_count:
            return remote(mix.at[block], cmix.at[j], sc.at[j, k], rc.at[j, k], me, other)
        return remote(parts.at[block, chunk(k)], cbuf.at[j, k], sc.at[j, k], rc.at[j, k], me, other)

    def across(k, j):
        to = toward(j) * 2 + side
        if k == ep_count:
            return remote(ysmix.at[j], ymix.at[j], sy.at[j, k], ry.at[j, k], me, to)
        return remote(ysend.at[j, k], ybuf.at[j, k], sy.at[j, k], ry.at[j, k], me, to)

    def home(k):
        return remote(abuf.at[k], returned.at[me], sa.at[k], ra.at[k], chunk(k), tp)

    wide = jnp.float32
    everything = order + [ep_count]
    for k in everything:
        for j in list(range(1, pairs)) + [0]:
            beside(k, j).start()
    for k in everything:
        for j in range(1, pairs):
            beside(k, j).wait_recv()
            block = toward(j) * 2 + side
            if k == ep_count:
                ysmix[j] = (mix[block].astype(wide) + cmix[j].astype(wide)).astype(mix.dtype)
            else:
                ysend[j, k] = (
                    parts[block, chunk(k)].astype(wide) + cbuf[j, k].astype(wide)
                ).astype(parts.dtype)
            across(k, j).start()
    for k in everything:
        beside(k, 0).wait_recv()
        if k == ep_count:
            total = mix[tp].astype(wide) + cmix[0].astype(wide)
        else:
            total = parts[tp, chunk(k)].astype(wide) + cbuf[0, k].astype(wide)
        for j in range(1, pairs):
            across(k, j).wait_recv()
            total = total + (ymix[j] if k == ep_count else ybuf[j, k]).astype(wide)
        total = total.astype(parts.dtype)
        if k == ep_count:
            mixed[...] = total
        elif k == 0:
            returned[me] = total
        else:
            abuf[k] = total
            home(k).start()
    for k in everything:
        for j in range(pairs):
            beside(k, j).wait_send()
            if j:
                across(k, j).wait_send()
        if 0 < k < ep_count:
            home(k).wait()


def give_back(parts, mix, ep_count, tp_count):
    pairs = tp_count // 2
    dma = pltpu.SemaphoreType.DMA
    vmem = pl.BlockSpec(memory_space=pltpu.VMEM)
    chunks, rows = parts.shape[1:], mix.shape[1:]
    many = (pairs, ep_count + 1)
    kind = parts.dtype
    return pl.pallas_call(
        functools.partial(return_kernel, ep_count, tp_count),
        out_shape=(
            jax.ShapeDtypeStruct(rows, kind),
            jax.ShapeDtypeStruct(chunks, kind),
        ),
        in_specs=[vmem] * 2,
        out_specs=(vmem, vmem),
        scratch_shapes=[
            pltpu.VMEM((pairs,) + chunks, kind),
            pltpu.VMEM((pairs,) + rows, kind),
            pltpu.VMEM((pairs,) + chunks, kind),
            pltpu.VMEM((pairs,) + rows, kind),
            pltpu.VMEM((pairs,) + chunks, kind),
            pltpu.VMEM((pairs,) + rows, kind),
            pltpu.VMEM(chunks, kind),
            dma(many),
            dma(many),
            dma(many),
            dma(many),
            dma((ep_count,)),
            dma((ep_count,)),
        ],
        compiler_params=pltpu.CompilerParams(collective_id=1, has_side_effects=True),
    )(parts, mix)


def per_device(
    recurrence_query,
    forget_preactivation,
    recurrence_value,
    output_gate_preactivation,
    forget_margin,
    surge_log_decay,
    head_norm_gain,
    recurrence_output_matrix,
    second_micro_input,
    expert_norm_gain,
    routes,
    router_chosen_logits,
    expert_gate_matrix,
    expert_up_matrix,
    expert_down_matrix,
):
    number_of_heads = surge_log_decay.shape[0]
    seq_len = recurrence_query.shape[0]
    tp_count = lax.axis_size("tp")
    expert_count = lax.axis_size("ep")
    tok_rows, width = second_micro_input.shape
    capacity = 2 * tok_rows * TOP // expert_count
    small = (
        recurrence_query,
        forget_preactivation,
        recurrence_value,
        output_gate_preactivation,
        forget_margin[None, :],
        surge_log_decay,
        head_norm_gain[None, :],
        second_micro_input,
        expert_norm_gain[None, :],
        routes,
        router_chosen_logits,
    )
    hidden_b, hidden_a, weights = dispatch(
        small,
        expert_gate_matrix[0].T,
        expert_up_matrix[0].T,
        number_of_heads,
        capacity,
        expert_count,
        tp_count,
    )
    hidden_b = hidden_b.reshape(-1, hidden_b.shape[-1])
    mix_rows = seq_len // tp_count
    mix_parts = jnp.dot(
        hidden_a, recurrence_output_matrix, preferred_element_type=jnp.float32
    ).astype(jnp.bfloat16)
    expert_parts = jnp.dot(
        hidden_b, expert_down_matrix[0], preferred_element_type=jnp.float32
    ).astype(jnp.bfloat16)
    mixed, returned = give_back(
        expert_parts.reshape(tp_count, expert_count, capacity, width),
        mix_parts.reshape(tp_count, mix_rows, width),
        expert_count,
        tp_count,
    )
    moe_out = jnp.dot(
        weights, returned.reshape(-1, width).astype(jnp.float32), precision=highest
    )
    return (mixed, moe_out.astype(jnp.bfloat16))


def solution(mesh):
    return jax.shard_map(
        per_device,
        mesh=mesh,
        in_specs=(
            P("ep", "tp"),
            P("ep", "tp"),
            P("ep", "tp"),
            P("ep", "tp"),
            P("tp"),
            P("tp", "ep"),
            P("tp"),
            P("tp", None),
            P(("ep", "tp"), None),
            P(),
            P("ep", None),
            P(("ep", "tp"), None),
            P("ep", None, "tp"),
            P("ep", None, "tp"),
            P("ep", "tp", None),
        ),
        out_specs=(P(("ep", "tp"), None), P(("ep", "tp"), None)),
        check_vma=False,
    )
```

profile of v0, /device:TPU:0, one launch (start us, length us, event | category | flops | bytes accessed | tf_op | source)
XLA Modules:
  0.0 111.5 jit_solution(1285360929548897595)
XLA Ops:
  0.6 0.0 copy-start
  0.6 1.5 %copy.18.logits_ref = f32[32,2]{1,0:T(8,128)} copy(f32[32,2]{0,1:T(2,128)} %param.26) | data formatting | bytes 512 | tf_op args[11]
  2.2 1.4 %copy.17.routes_ref = s32[128,2]{1,0:T(8,128)} copy(s32[128,2]{0,1:T(2,128)} %param.25) | data formatting | bytes 2048 | tf_op args[10]
  3.6 54.3 %shard_map.158 = (bf16[4,128,352]{2,1,0:T(8,128)(2,1)}, bf16[128,256]{1,0:T(8,128)(2,1)}, f32[32,128]{1,0:T(8,128)}) custom-call(bf16[128,256]{1,0:T(8,128)(2,1)} %query_ref.1, bf16[128,256]{1,0:T(8,128)(2,1)} %forget_ref.1, bf16[128,256]{1,0:T(8,128)(2,1)} %value_ref.1, bf16[128,256]{1,0:T(8,128)(2,1)} %opening_ref.1, f32[1,256]{1,0:T(1,128)} %bitcast.27, ...), custom_call_target="tpu_custom_call" | custom-call | tf_op jit(solution)/shard_map/pallas_call | solution.py:340
  57.9 0.0 copy-start.2
  57.9 3.1 %convolution_convert_fusion.1 = bf16[128,4096]{1,0:T(8,128)(2,1)} fusion(bf16[128,256]{1,0:T(8,128)(2,1)} %get-tuple-element.8, bf16[256,4096]{1,0:T(8,128)(2,1)} %param.22), kind=kOutput, calls=%fused_computation.1 | convolution fusion | flops 268959744 | bytes 3211264 | tf_op jit(solution)/shard_map/dot_general | solution.py:560
  61.1 0.0 copy-done
  61.1 0.0 copy-done.2
  61.1 4.3 %convolution_convert_fusion = bf16[512,4096]{1,0:T(8,128)(2,1)} fusion(bf16[512,352]{1,0:T(8,128)(2,1)S(1)} %bitcast.29, bf16[1,352,4096]{2,1,0:T(8,128)(2,1)S(1)} %copy-done), kind=kOutput, calls=%fused_computation | convolution fusion | flops 1478492160 | bytes 7438336 | tf_op jit(solution)/shard_map/dot_general | solution.py:563
  65.3 0.0 copy-start.1
  65.3 42.0 %shard_map.159 = (bf16[32,4096]{1,0:T(8,128)(2,1)}, bf16[8,16,4096]{2,1,0:T(8,128)(2,1)}) custom-call(bf16[4,8,16,4096]{3,2,1,0:T(8,128)(2,1)} %bitcast.22, bf16[4,32,4096]{2,1,0:T(8,128)(2,1)} %bitcast.21), custom_call_target="tpu_custom_call" | custom-call | tf_op jit(solution)/shard_map/pallas_call | solution.py:486
  107.4 0.0 copy-done.1
  107.4 2.5 %convolution_convert_fusion.2 = bf16[32,4096]{1,0:T(8,128)(2,1)} fusion(f32[32,128]{1,0:T(8,128)S(1)} %copy-done.1, bf16[128,4096]{1,0:T(8,128)(2,1)} %bitcast.25), kind=kOutput, calls=%fused_computation.2 | convolution fusion | flops 201457664 | bytes 1327104 | tf_op jit(solution)/shard_map/dot_general | solution.py:572
  109.9 1.7 %copy.20 = bf16[32,4096]{1,0:T(8,128)(2,1)} copy(bf16[32,4096]{1,0:T(8,128)(2,1)} %get-tuple-element.14) | data formatting | bytes 524288
Async XLA Ops:
  0.6 60.4 %copy-start = (bf16[1,352,4096]{2,1,0:T(8,128)(2,1)S(1)}, bf16[1,352,4096]{2,1,0:T(8,128)(2,1)}, u32[]{:S(2)}) copy-start(bf16[1,352,4096]{2,1,0:T(8,128)(2,1)} %param.29) | copy-start | bytes 8650756
  57.9 3.1 %copy-start.2 = (bf16[4,128,352]{2,1,0:T(8,128)(2,1)S(1)}, bf16[4,128,352]{2,1,0:T(8,128)(2,1)}, u32[]{:S(2)}) copy-start(bf16[4,128,352]{2,1,0:T(8,128)(2,1)} %get-tuple-element.7) | copy-start | bytes 1081348
  65.3 42.0 %copy-start.1 = (f32[32,128]{1,0:T(8,128)S(1)}, f32[32,128]{1,0:T(8,128)}, u32[]{:S(2)}) copy-start(f32[32,128]{1,0:T(8,128)} %get-tuple-element.10) | copy-start | bytes 49156
where the time goes:
time: 112 us
  Pallas kernels  96.4 us (86%)
  matrix products  9.86 us (9%)
  local copies, waits for them, and re-layouts  4.61 us (4%)
    pallas_call x1, Pallas kernels, dispatch(): pl.pallas_call(functools.partial(dispatch_kernel, ep_count, tp_count), ou...  54.3 us
    pallas_call x1, Pallas kernels, give_back(): pl.pallas_call(functools.partial(return_kernel, ep_count, tp_count), out_...  42 us
    unnamed x9, local copies, waits for them, and re-layouts  4.61 us
    dot_general x1, matrix products, per_device(): jnp.dot(hidden_b, expert_down_matrix[0], preferred_element_type=jnp.float32)  4.28 us
    dot_general x1, matrix products, per_device(): jnp.dot(hidden_a, recurrence_output_matrix, preferred_element_type=jnp.fl...  3.11 us
    dot_general x1, matrix products, per_device(): jnp.dot(weights, returned.reshape(-1, width).astype(jnp.float32), precisi...  2.46 us

commit v1 on v0

v1 whole, which is shorter than its diff:
```python
import functools

import jax
import jax.numpy as jnp
from jax import lax
from jax.experimental import pallas as pl
from jax.experimental.pallas import tpu as pltpu
from jax.sharding import PartitionSpec as P

TOP = 2
SPAN = 64
MESH = pl.DeviceIdType.MESH


epsilon = 1e-06
wide = jnp.float32
kind = jnp.bfloat16


def visiting_order(count):
    half = count // 2
    near = [(i / max(1, half - 1), i + 1) for i in range(half - 1)]
    far = [((i + 0.9) / half, half + i) for i in range(half)]
    return [0] + [k for _, k in sorted(near + far)]


def mate(me, k, count):
    found, bit = me, 1
    while bit < count:
        if k & bit:
            found = found + bit * (1 - 2 * lax.rem(lax.div(me, bit), 2))
        bit *= 2
    return found


def greet(me, tp, ep_count, tp_count):
    pairs = tp_count // 2
    pair, side = tp // 2, tp % 2
    barrier = pltpu.get_barrier_semaphore()
    for k in range(1, ep_count):
        pl.semaphore_signal(
            barrier,
            inc=1,
            device_id={"ep": lax.rem(me + k, ep_count), "tp": tp},
            device_id_type=MESH,
        )
    for j in range(1, pairs):
        pl.semaphore_signal(
            barrier,
            inc=1,
            device_id={"ep": me, "tp": lax.rem(pair + j, pairs) * 2 + side},
            device_id_type=MESH,
        )
    pl.semaphore_signal(
        barrier, inc=1, device_id={"ep": me, "tp": pair * 2 + 1 - side}, device_id_type=MESH
    )


def product(left, right, left_axis, right_axis):
    return lax.dot_general(
        left,
        right,
        (((left_axis,), (right_axis,)), ((), ())),
        preferred_element_type=wide,
    )


def iota(shape, axis):
    return lax.broadcasted_iota(jnp.int32, shape, axis)


def thirds(array):
    high = array.astype(kind)
    rest = array - high.astype(wide)
    middle = rest.astype(kind)
    return [high, middle, (rest - middle.astype(wide)).astype(kind)]


def kernel(
    ep_count,
    tp_count,
    query_ref,
    forget_ref,
    value_ref,
    opening_ref,
    margin_ref,
    surge_ref,
    head_gain_ref,
    tokens_ref,
    gain_ref,
    routes_ref,
    logits_ref,
    gate_hbm,
    up_hbm,
    down_hbm,
    matrix_hbm,
    mixed_ref,
    moe_ref,
    slots,
    piece,
    both,
    down,
    matrix,
    weights,
    lifted_ref,
    local_ref,
    window,
    window_total,
    before,
    before_total,
    outgoing,
    incoming,
    parts,
    mix,
    cbuf,
    cmix,
    ysend,
    ysmix,
    ybuf,
    ymix,
    abuf,
    returned,
    load,
    sa,
    ra,
    sy,
    ry,
    sc,
    rc,
    ss,
    rs,
    sb,
    rb,
    sz,
    rz,
    sh,
    rh,
):
    me, tp = lax.axis_index("ep"), lax.axis_index("tp")
    pairs = tp_count // 2
    pair, side = tp // 2, tp % 2
    other = pair * 2 + 1 - side
    order = visiting_order(ep_count)
    heads, seq_len = surge_ref.shape
    key_width = query_ref.shape[1] // heads
    value_width = value_ref.shape[1] // heads
    tok_rows, width = tokens_ref.shape
    capacity = slots.shape[1]
    units = gate_hbm.shape[0]
    offset = both.shape[0] // 2
    mix_rows = mix.shape[1]
    steps = outgoing.shape[0]
    half = ep_count * 5 // 8
    first, second = list(range(half)), list(range(half, ep_count))
    extra = ep_count
    whole_tiles = capacity % 16 == 0
    stride = min(width, 1024) if whole_tiles else width

    greet(me, tp, ep_count, tp_count)
    fetch = [
        pltpu.make_async_copy(gate_hbm, both.at[pl.ds(0, units)], load.at[0]),
        pltpu.make_async_copy(up_hbm, both.at[pl.ds(offset, units)], load.at[1]),
        pltpu.make_async_copy(down_hbm, down, load.at[2]),
        pltpu.make_async_copy(matrix_hbm, matrix, load.at[3]),
    ]
    for copy in fetch:
        copy.start()

    def remote(src, dst, send, recv, ep, to):
        return pltpu.make_async_remote_copy(
            src_ref=src,
            dst_ref=dst,
            send_sem=send,
            recv_sem=recv,
            device_id={"ep": ep, "tp": to},
            device_id_type=MESH,
        )

    def toward(j):
        return lax.rem(pair + j, pairs)

    def exchange(i):
        to = mate(me, order[i], ep_count)
        return remote(slots.at[i], piece.at[i, tp], sa.at[i], ra.at[i], to, tp)

    def across(i, j):
        to = toward(j) * 2 + side
        return remote(piece.at[i, tp], piece.at[i, tp], sy.at[j, i], ry.at[j, i], me, to)

    def beside(i, j):
        block = lax.rem(pair + pairs - j, pairs) * 2 + side
        return remote(
            piece.at[i, block], piece.at[i, block], sc.at[j, i], rc.at[j, i], me, other
        )

    def back_beside(i, j):
        block = toward(j) * 2 + 1 - side
        if i == extra:
            return remote(mix.at[block], cmix.at[j], sb.at[j, i], rb.at[j, i], me, other)
        return remote(parts.at[i, block], cbuf.at[j, i], sb.at[j, i], rb.at[j, i], me, other)

    def back_across(i, j):
        to = toward(j) * 2 + side
        if i == extra:
            return remote(ysmix.at[j], ymix.at[j], sz.at[j, i], rz.at[j, i], me, to)
        return remote(ysend.at[j, i], ybuf.at[j, i], sz.at[j, i], rz.at[j, i], me, to)

    def home(i):
        to = mate(me, order[i], ep_count)
        return remote(abuf.at[i], returned.at[i], sh.at[i], rh.at[i], to, tp)

    def pass_on(i):
        for j in range(1, pairs):
            across(i, j).start()
        beside(i, 0).start()

    def forward(i):
        exchange(i).wait_recv()
        pass_on(i)

    def relay(i):
        for j in range(1, pairs):
            across(i, j).wait_recv()
            beside(i, j).start()

    rows = tokens_ref[...].astype(wide)
    normed = (
        rows * lax.rsqrt(jnp.mean(rows * rows, axis=-1, keepdims=True) + epsilon) * gain_ref[...]
    ).astype(kind)
    listed = routes_ref[...]
    routes = listed[:, :tok_rows]
    for t in range(1, tp_count):
        routes = jnp.where(tp == t, listed[:, t * tok_rows : (t + 1) * tok_rows], routes)
    named = [routes[i : i + 1, :] for i in range(TOP)]
    experts = iota((ep_count, tok_rows), 0)
    tables = [(row == experts).astype(wide) for row in named]
    strict = (iota((tok_rows, tok_rows), 0) < iota((tok_rows, tok_rows), 1)).astype(kind)
    earlier = product(sum(tables).astype(kind), strict, 1, 0)
    places = [jnp.sum(earlier * table, axis=0, keepdims=True) for table in tables]
    spots = [row * capacity + place.astype(jnp.int32) for row, place in zip(named, places)]
    logits = logits_ref[...]
    raised = jnp.exp(logits - jnp.max(logits, axis=0, keepdims=True))
    share = raised / jnp.sum(raised, axis=0, keepdims=True)
    places_of = [
        iota((capacity, tok_rows), 0) + mate(me, k, ep_count) * capacity for k in order
    ]
    if whole_tiles:
        wanted = jnp.concatenate(places_of, axis=0)
        chooser = sum((spot == wanted).astype(wide) for spot in spots).astype(kind)
        for c in range(0, width, stride):
            cut = slice(c, c + stride)
            chosen = product(chooser, normed[:, cut], 1, 0).astype(kind)
            piece[0, tp, :, cut] = chosen[:capacity]
            for i in range(1, ep_count):
                slots[i, :, cut] = chosen[i * capacity : (i + 1) * capacity]
    else:
        for i, wanted in enumerate(places_of):
            chooser = sum((spot == wanted).astype(wide) for spot in spots).astype(kind)
            chosen = product(chooser, normed, 1, 0).astype(kind)
            if i:
                slots[i] = chosen
            else:
                piece[0, tp] = chosen
    pl.semaphore_wait(pltpu.get_barrier_semaphore(), ep_count + pairs - 1)
    pass_on(0)
    for i in range(1, ep_count):
        exchange(i).start()

    for i, wanted in enumerate(places_of):
        weight = sum(
            jnp.where(spot == wanted, share[r : r + 1, :], 0.0) for r, spot in enumerate(spots)
        )
        high = weight.astype(kind)
        low = (weight - high.astype(wide)).astype(kind)
        weights[0, i * capacity : (i + 1) * capacity, :] = high
        weights[1, i * capacity : (i + 1) * capacity, :] = low
    if units < offset:
        both[units:offset, :] = jnp.zeros((offset - units, width), kind)
        both[offset + units :, :] = jnp.zeros((offset - units, width), kind)

    at, since = iota((seq_len, seq_len), 0), iota((seq_len, seq_len), 1)
    shut = jax.nn.sigmoid(-forget_ref[...].astype(wide)) * margin_ref[...]
    within = ((at >= since) & (at // SPAN == since // SPAN)).astype(wide)
    running_all = sum(
        product(within.astype(kind), part, 1, 0) for part in thirds(jnp.log1p(-shut))
    )
    triangle = iota((SPAN, SPAN), 0) >= iota((SPAN, SPAN), 1)

    def recur(head):
        keys = slice(head * key_width, (head + 1) * key_width)
        values = slice(head * value_width, (head + 1) * value_width)
        surges = jnp.sum(within * surge_ref[head : head + 1, :], axis=1, keepdims=True)
        running_head = running_all[:, keys] + surges
        state = jnp.zeros((value_width, key_width), wide)
        total = jnp.zeros((1, key_width), wide)
        for span in range(seq_len // SPAN):
            part = slice(span * SPAN, (span + 1) * SPAN)
            running = running_head[part]
            closing = running[SPAN - 1 : SPAN]
            inflow = shut[part, keys]
            value = value_ref[part, values]
            query = query_ref[part, keys].astype(wide)
            lifted = (query * jnp.exp(running)).astype(kind)
            lowered = (inflow * jnp.exp(-running)).astype(kind)
            scores = jnp.where(triangle, product(lifted, lowered, 1, 1), 0.0)
            local = product(scores.astype(kind), value, 1, 0)
            if span:
                local = local + product(lifted, state.astype(kind), 1, 1)
            local_ref[part, values] = local
            lifted_ref[part, keys] = (query * jnp.exp(running + total)).astype(kind)
            fresh = product(value, (inflow * jnp.exp(closing - running)).astype(kind), 0, 0)
            state = jnp.exp(closing) * state + fresh
            total = total + closing
        window[head] = state
        window_total[head] = total

    def state_copy(step):
        to = lax.rem(me + 2**step, ep_count)
        return remote(outgoing.at[step], incoming.at[step], ss.at[step], rs.at[step], to, tp)

    def send_window(step):
        for head in range(heads):
            outgoing[step, head, :value_width] = window[head].astype(kind)
            total = window_total[head]
            coarse = total.astype(kind).astype(wide)
            line = iota((16, key_width), 0)
            tail = jnp.where(line == 0, coarse, jnp.where(line == 1, total - coarse, 0.0))
            outgoing[step, head, value_width:] = tail.astype(kind)

        @pl.when(me + 2**step < ep_count)
        def _():
            state_copy(step).start()

    def take_window(step):
        @pl.when(me >= 2**step)
        def _():
            state_copy(step).wait_recv()
            for head in range(heads):
                state = incoming[step, head, :value_width].astype(wide)
                total = jnp.sum(
                    incoming[step, head, value_width:].astype(wide), axis=0, keepdims=True
                )
                before[head] = jnp.exp(before_total[head]) * state + before[head]
                before_total[head] = before_total[head] + total
                window[head] = jnp.exp(window_total[head]) * state + window[head]
                window_total[head] = window_total[head] + total

    scanned = []

    def scan():
        if len(scanned) < steps:
            take_window(len(scanned))
            scanned.append(0)
            if len(scanned) < steps:
                send_window(len(scanned))

    def gathered(ref, group, sources=None):
        start, stop = group[0], group[-1] + 1
        if whole_tiles:
            return ref[start:stop].reshape(-1, width)
        if len(ref.shape) == 3:
            return jnp.concatenate([ref[i] for i in group], axis=0)
        return jnp.concatenate([ref[i, t] for i in group for t in range(tp_count)], axis=0)

    def arrive(group):
        for i in group:
            for j in range(pairs):
                beside(i, j).wait_recv()

    def raise_hidden(group):
        result = product(gathered(piece, group), both[...], 1, 1)
        left, right = result[:, :units], result[:, offset : offset + units]
        return (left * jax.nn.sigmoid(left) * right).astype(kind)

    def lower_hidden(group, hidden):
        start, stop = group[0], group[-1] + 1
        for c in range(0, width, stride):
            cut = slice(c, c + stride)
            result = product(hidden, down[:, cut], 1, 0).astype(kind)
            if whole_tiles:
                parts[start:stop, :, :, cut] = result.reshape(
                    stop - start, tp_count, capacity, stride
                )
            else:
                for n in range((stop - start) * tp_count):
                    i, t = start + n // tp_count, n % tp_count
                    parts[i, t, :, cut] = result[n * capacity : (n + 1) * capacity]

    def leaving(group):
        return sorted(group, key=lambda i: -order[i])

    def hand_over(group):
        for i in group:
            for j in list(range(1, pairs)) + [0]:
                back_beside(i, j).start()

    def fold(i):
        for j in range(1, pairs):
            back_beside(i, j).wait_recv()
            block = toward(j) * 2 + side
            if i == extra:
                ysmix[j] = (mix[block].astype(wide) + cmix[j].astype(wide)).astype(kind)
            else:
                ysend[j, i] = (parts[i, block].astype(wide) + cbuf[j, i].astype(wide)).astype(
                    kind
                )
            back_across(i, j).start()

    def settle(i):
        back_beside(i, 0).wait_recv()
        if i == extra:
            total = mix[tp].astype(wide) + cmix[0].astype(wide)
        else:
            total = parts[i, tp].astype(wide) + cbuf[0, i].astype(wide)
        for j in range(1, pairs):
            back_across(i, j).wait_recv()
            total = total + (ymix[j] if i == extra else ybuf[j, i]).astype(wide)
        total = total.astype(kind)
        if i == extra:
            mixed_ref[...] = total
        elif i == 0:
            returned[0] = total
        else:
            abuf[i] = total
            home(i).start()

    def combine(group):
        start, stop = group[0] * capacity, (group[-1] + 1) * capacity
        taken = gathered(returned, group)
        return product(weights[0, start:stop], taken, 0, 0) + product(
            weights[1, start:stop], taken, 0, 0
        )

    spare = len(second)
    quarter = max(1, spare // 4)
    chunks = [second[n : n + quarter] for n in range(0, spare, quarter)]

    def advance(group):
        for i in group:
            forward(i)
            relay(i - 1)

    recur(0)
    advance(first[1:2])
    for head in range(1, heads):
        recur(head)
    before[...] = jnp.zeros_like(before)
    before_total[...] = jnp.zeros_like(before_total)
    send_window(0)
    advance(first[2:])
    advance(chunks[0])
    arrive(first)
    for copy in fetch[:3]:
        copy.wait()
    hidden = raise_hidden(first)
    for chunk in chunks[1:2]:
        advance(chunk)
    scan()
    lower_hidden(first, hidden)
    hand_over(leaving(first))
    for chunk in chunks[2:]:
        advance(chunk)
    for i in leaving(first):
        fold(i)
    relay(ep_count - 1)
    scan()
    arrive(second)
    hidden = raise_hidden(second)
    lower_hidden(second, hidden)
    hand_over(leaving(second))
    for i in leaving(first)[:2]:
        settle(i)
    for i in leaving(second):
        fold(i)
    for _ in range(steps):
        scan()
    for head in range(heads):
        keys = slice(head * key_width, (head + 1) * key_width)
        values = slice(head * value_width, (head + 1) * value_width)
        out = local_ref[:, values] + product(
            lifted_ref[:, keys], before[head].astype(kind), 1, 1
        )
        out = out * lax.rsqrt(jnp.mean(out * out, axis=-1, keepdims=True) + epsilon)
        opening = opening_ref[:, values].astype(wide)
        lifted_ref[:, values] = (
            out * head_gain_ref[:, values] * (opening * jax.nn.sigmoid(opening))
        ).astype(kind)
    fetch[3].wait()
    for c in range(0, width, stride):
        cut = slice(c, c + stride)
        result = product(lifted_ref[...], matrix[:, cut], 1, 0).astype(kind)
        mix[:, :, cut] = result.reshape(tp_count, mix_rows, stride)
    hand_over([extra])
    for i in leaving(first)[2:]:
        settle(i)
    fold(extra)
    for i in leaving(second):
        settle(i)
    for i in first[1:]:
        home(i).wait_recv()
    total = combine(first)
    for i in second:
        home(i).wait_recv()
    moe_ref[...] = (total + combine(second)).astype(kind)
    settle(extra)

    for i in range(ep_count):
        if i:
            exchange(i).wait_send()
            home(i).wait_send()
    for i in range(ep_count + 1):
        for j in range(pairs):
            back_beside(i, j).wait_send()
            if j:
                back_across(i, j).wait_send()
            if i < ep_count:
                beside(i, j).wait_send()
                if j:
                    across(i, j).wait_send()
    for step in range(steps):

        @pl.when(me + 2**step < ep_count)
        def _(step=step):
            state_copy(step).wait_send()


def run(small, large, heads, capacity, ep_count, tp_count):
    pairs = tp_count // 2
    dma = pltpu.SemaphoreType.DMA
    vmem = pl.BlockSpec(memory_space=pltpu.VMEM)
    hbm = pl.BlockSpec(memory_space=pl.ANY)
    query, value, tokens = small[0], small[2], small[7]
    gate, _, down, matrix = large
    seq_len, keys = query.shape
    values = value.shape[1]
    tok_rows, width = tokens.shape
    units = gate.shape[0]
    padded = -(-units // 128) * 128
    key_width, value_width = keys // heads, values // heads
    steps = (ep_count - 1).bit_length()
    mix_rows = seq_len // tp_count
    chunks = (ep_count, capacity, width)
    many = (pairs, ep_count + 1)
    state = (steps, heads, value_width + 16, key_width)
    return pl.pallas_call(
        functools.partial(kernel, ep_count, tp_count),
        out_shape=(
            jax.ShapeDtypeStruct((mix_rows, width), kind),
            jax.ShapeDtypeStruct((tok_rows, width), kind),
        ),
        in_specs=[vmem] * len(small) + [hbm] * len(large),
        out_specs=(vmem, vmem),
        scratch_shapes=[
            pltpu.VMEM(chunks, kind),
            pltpu.VMEM((ep_count, tp_count, capacity, width), kind),
            pltpu.VMEM((2 * padded, width), kind),
            pltpu.VMEM(down.shape, kind),
            pltpu.VMEM(matrix.shape, kind),
            pltpu.VMEM((2, ep_count * capacity, tok_rows), kind),
            pltpu.VMEM((seq_len, keys), kind),
            pltpu.VMEM((seq_len, values), wide),
            pltpu.VMEM((heads, value_width, key_width), wide),
            pltpu.VMEM((heads, 1, key_width), wide),
            pltpu.VMEM((heads, value_width, key_width), wide),
            pltpu.VMEM((heads, 1, key_width), wide),
            pltpu.VMEM(state, kind),
            pltpu.VMEM(state, kind),
            pltpu.VMEM((ep_count, tp_count, capacity, width), kind),
            pltpu.VMEM((tp_count, mix_rows, width), kind),
            pltpu.VMEM((pairs,) + chunks, kind),
            pltpu.VMEM((pairs, mix_rows, width), kind),
            pltpu.VMEM((pairs,) + chunks, kind),
            pltpu.VMEM((pairs, mix_rows, width), kind),
            pltpu.VMEM((pairs,) + chunks, kind),
            pltpu.VMEM((pairs, mix_rows, width), kind),
            pltpu.VMEM(chunks, kind),
            pltpu.VMEM(chunks, kind),
            dma((4,)),
            dma((ep_count,)),
            dma((ep_count,)),
            dma(many),
            dma(many),
            dma(many),
            dma(many),
            dma((steps,)),
            dma((steps,)),
            dma(many),
            dma(many),
            dma(many),
            dma(many),
            dma((ep_count,)),
            dma((ep_count,)),
        ],
        compiler_params=pltpu.CompilerParams(
            collective_id=0, has_side_effects=True, vmem_limit_bytes=60 << 20
        ),
    )(*small, *large)


def per_device(
    recurrence_query,
    forget_preactivation,
    recurrence_value,
    output_gate_preactivation,
    forget_margin,
    surge_log_decay,
    head_norm_gain,
    recurrence_output_matrix,
    second_micro_input,
    expert_norm_gain,
    routes,
    router_chosen_logits,
    expert_gate_matrix,
    expert_up_matrix,
    expert_down_matrix,
):
    tp_count = lax.axis_size("tp")
    expert_count = lax.axis_size("ep")
    tok_rows = second_micro_input.shape[0]
    capacity = 2 * tok_rows * TOP // expert_count
    small = (
        recurrence_query,
        forget_preactivation,
        recurrence_value,
        output_gate_preactivation,
        forget_margin[None, :],
        surge_log_decay,
        head_norm_gain[None, :],
        second_micro_input,
        expert_norm_gain[None, :],
        routes.T,
        router_chosen_logits.T,
    )
    large = (
        expert_gate_matrix[0].T,
        expert_up_matrix[0].T,
        expert_down_matrix[0],
        recurrence_output_matrix,
    )
    return run(small, large, surge_log_decay.shape[0], capacity, expert_count, tp_count)


def solution(mesh):
    return jax.shard_map(
        per_device,
        mesh=mesh,
        in_specs=(
            P("ep", "tp"),
            P("ep", "tp"),
            P("ep", "tp"),
            P("ep", "tp"),
            P("tp"),
            P("tp", "ep"),
            P("tp"),
            P("tp", None),
            P(("ep", "tp"), None),
            P(),
            P("ep", None),
            P(("ep", "tp"), None),
            P("ep", None, "tp"),
            P("ep", None, "tp"),
            P("ep", "tp", None),
        ),
        out_specs=(P(("ep", "tp"), None), P(("ep", "tp"), None)),
        check_vma=False,
    )
```

time: 112 us -> 74.6 us (0.67)
  Pallas kernels: 96.4 us -> 69.3 us
  matrix products: 9.86 us -> 0 us
  local copies, waits for them, and re-layouts: 4.61 us -> 3.34 us
    pallas_call x2 -> x1, Pallas kernels: 96.4 us -> 69.3 us  [run(): pl.pallas_call(functools.partial(kernel, ep_count, tp_count), out_shape=(...]
    dot_general x3 -> x0, matrix products: 9.86 us -> none  [the longest x1 4.28 us: per_device(): jnp.dot(hidden_b, expert_down_matrix[0], preferred_element_type=jnp.float32)]
    unnamed x9 -> x2, local copies, waits for them, and re-layouts: 4.61 us -> 3.34 us
where the time goes in v1:
time: 74.6 us; the launch traced here: 73.3 us
  Pallas kernels  69.3 us (93%)
  local copies, waits for them, and re-layouts  3.34 us (4%)
    pallas_call x1, Pallas kernels, run(): pl.pallas_call(functools.partial(kernel, ep_count, tp_count), out_shape=(...  69.3 us
    unnamed x2, local copies, waits for them, and re-layouts  3.34 us

profile of v1, /device:TPU:0, one launch (start us, length us, event | category | flops | bytes accessed | tf_op | source)
XLA Modules:
  0.0 73.3 jit_solution(4203452560943361282)
XLA Ops:
  0.6 69.3 %shard_map.158 = (bf16[32,4096]{1,0:T(8,128)(2,1)}, bf16[32,4096]{1,0:T(8,128)(2,1)}) custom-call(bf16[128,256]{1,0:T(8,128)(2,1)} %query_ref.1, bf16[128,256]{1,0:T(8,128)(2,1)} %forget_ref.1, bf16[128,256]{1,0:T(8,128)(2,1)} %value_ref.1, bf16[128,256]{1,0:T(8,128)(2,1)} %opening_ref.1, f32[1,256]{1,0:T(1,128)} %bitcast.16, f32[2,128]{1,0:T(2,128)} %surge_ref.1, ...), custom_call_target="tpu_custom_call" | custom-call | tf_op jit(solution)/shard_map/pallas_call | solution.py:545
  70.0 1.7 %copy.19 = bf16[32,4096]{1,0:T(8,128)(2,1)} copy(bf16[32,4096]{1,0:T(8,128)(2,1)} %get-tuple-element.4) | data formatting | bytes 524288
  71.6 1.7 %copy.20 = bf16[32,4096]{1,0:T(8,128)(2,1)} copy(bf16[32,4096]{1,0:T(8,128)(2,1)} %get-tuple-element.5) | data formatting | bytes 524288

commit v2 on v1

--- a/solution.py
+++ b/solution.py
@@ -99,9 +99,13 @@
     slots,
     piece,
     both,
+    turned,
     down,
     matrix,
     weights,
+    note,
+    notes,
+    guest_weights,
     lifted_ref,
     local_ref,
     window,
@@ -120,6 +124,10 @@
     ymix,
     abuf,
     returned,
+    guest_abuf,
+    guest_returned,
+    crossing,
+    crossed,
     load,
     sa,
     ra,
@@ -135,6 +143,12 @@
     rz,
     sh,
     rh,
+    sg,
+    rg,
+    sn,
+    rn,
+    su,
+    ru,
 ):
     me, tp = lax.axis_index("ep"), lax.axis_index("tp")
     pairs = tp_count // 2
@@ -150,9 +164,11 @@
     offset = both.shape[0] // 2
     mix_rows = mix.shape[1]
     steps = outgoing.shape[0]
-    half = ep_count * 5 // 8
-    first, second = list(range(half)), list(range(half, ep_count))
+    cuts = (0, ep_count // 2, ep_count * 7 // 8, ep_count)
+    first, second, third = [list(range(*cuts[n : n + 2])) for n in range(3)]
     extra = ep_count
+    near = [i for i in range(ep_count) if 2 * order[i] < ep_count]
+    distant = [i for i in range(ep_count) if i not in near]
     whole_tiles = capacity % 16 == 0
     stride = min(width, 1024) if whole_tiles else width
 
@@ -209,6 +225,36 @@
         to = mate(me, order[i], ep_count)
         return remote(abuf.at[i], returned.at[i], sh.at[i], rh.at[i], to, tp)
 
+    def tell(j):
+        return remote(note, notes.at[j], sn.at[j], rn.at[j], me, toward(j) * 2 + side)
+
+    def home_guest(i, j):
+        to = mate(me, order[i], ep_count)
+        at = near.index(i)
+        return remote(
+            guest_abuf.at[j, at], guest_returned.at[j, at], sg.at[j, i], rg.at[j, i], to, tp
+        )
+
+    def cross(j):
+        to = toward(j) * 2 + side
+        return remote(crossing.at[j], crossed.at[j], su.at[j], ru.at[j], me, to)
+
+    def back_beside(i, j):
+        block = toward(j) * 2 + 1 - side
+        if i == extra:
+            return remote(mix.at[block], cmix.at[j], sb.at[j, i], rb.at[j, i], me, other)
+        return remote(parts.at[i, block], cbuf.at[j, i], sb.at[j, i], rb.at[j, i], me, other)
+
+    def back_across(i, j):
+        to = toward(j) * 2 + side
+        if i == extra:
+            return remote(ysmix.at[j], ymix.at[j], sz.at[j, i], rz.at[j, i], me, to)
+        return remote(ysend.at[j, i], ybuf.at[j, i], sz.at[j, i], rz.at[j, i], me, to)
+
+    def home(i):
+        to = mate(me, order[i], ep_count)
+        return remote(abuf.at[i], returned.at[i], sh.at[i], rh.at[i], to, tp)
+
     def pass_on(i):
         for j in range(1, pairs):
             across(i, j).start()
@@ -228,52 +274,72 @@
         rows * lax.rsqrt(jnp.mean(rows * rows, axis=-1, keepdims=True) + epsilon) * gain_ref[...]
     ).astype(kind)
     listed = routes_ref[...]
-    routes = listed[:, :tok_rows]
-    for t in range(1, tp_count):
-        routes = jnp.where(tp == t, listed[:, t * tok_rows : (t + 1) * tok_rows], routes)
-    named = [routes[i : i + 1, :] for i in range(TOP)]
     experts = iota((ep_count, tok_rows), 0)
-    tables = [(row == experts).astype(wide) for row in named]
     strict = (iota((tok_rows, tok_rows), 0) < iota((tok_rows, tok_rows), 1)).astype(kind)
-    earlier = product(sum(tables).astype(kind), strict, 1, 0)
-    places = [jnp.sum(earlier * table, axis=0, keepdims=True) for table in tables]
-    spots = [row * capacity + place.astype(jnp.int32) for row, place in zip(named, places)]
-    logits = logits_ref[...]
-    raised = jnp.exp(logits - jnp.max(logits, axis=0, keepdims=True))
-    share = raised / jnp.sum(raised, axis=0, keepdims=True)
+
+    def spots_of(index):
+        routes = listed[:, :tok_rows]
+        for t in range(1, tp_count):
+            routes = jnp.where(index == t, listed[:, t * tok_rows : (t + 1) * tok_rows], routes)
+        named = [routes[i : i + 1, :] for i in range(TOP)]
+        tables = [(row == experts).astype(wide) for row in named]
+        earlier = product(sum(tables).astype(kind), strict, 1, 0)
+        places = [jnp.sum(earlier * table, axis=0, keepdims=True) for table in tables]
+        return [row * capacity + place.astype(jnp.int32) for row, place in zip(named, places)]
+
     places_of = [
         iota((capacity, tok_rows), 0) + mate(me, k, ep_count) * capacity for k in order
     ]
-    if whole_tiles:
-        wanted = jnp.concatenate(places_of, axis=0)
-        chooser = sum((spot == wanted).astype(wide) for spot in spots).astype(kind)
-        for c in range(0, width, stride):
-            cut = slice(c, c + stride)
-            chosen = product(chooser, normed[:, cut], 1, 0).astype(kind)
-            piece[0, tp, :, cut] = chosen[:capacity]
-            for i in range(1, ep_count):
-                slots[i, :, cut] = chosen[i * capacity : (i + 1) * capacity]
-    else:
-        for i, wanted in enumerate(places_of):
+
+    def choose(spots, tokens, members, store):
+        if whole_tiles:
+            wanted = jnp.concatenate([places_of[i] for i in members], axis=0)
             chooser = sum((spot == wanted).astype(wide) for spot in spots).astype(kind)
-            chosen = product(chooser, normed, 1, 0).astype(kind)
-            if i:
-                slots[i] = chosen
-            else:
-                piece[0, tp] = chosen
+            for c in range(0, width, stride):
+                cut = slice(c, c + stride)
+                chosen = product(chooser, tokens[:, cut], 1, 0).astype(kind)
+                for n, i in enumerate(members):
+                    store(i, cut, chosen[n * capacity : (n + 1) * capacity])
+        else:
+            for i in members:
+                chooser = sum((spot == places_of[i]).astype(wide) for spot in spots)
+                store(i, slice(None), product(chooser.astype(kind), tokens, 1, 0).astype(kind))
+
+    def keep(i, cut, rows):
+        if i:
+            slots[i, :, cut] = rows
+        else:
+            piece[i, tp, :, cut] = rows
+
+    spots = spots_of(tp)
+    choose(spots, normed, range(ep_count), keep)
     pl.semaphore_wait(pltpu.get_barrier_semaphore(), ep_count + pairs - 1)
     pass_on(0)
     for i in range(1, ep_count):
         exchange(i).start()
 
-    for i, wanted in enumerate(places_of):
-        weight = sum(
-            jnp.where(spot == wanted, share[r : r + 1, :], 0.0) for r, spot in enumerate(spots)
-        )
-        high = weight.astype(kind)
-        low = (weight - high.astype(wide)).astype(kind)
+    def share_of(logits):
+        raised = jnp.exp(logits - jnp.max(logits, axis=0, keepdims=True))
+        return raised / jnp.sum(raised, axis=0, keepdims=True)
+
+    def weigh(spots, share, members, store):
+        for i in members:
+            weight = sum(
+                jnp.where(spot == places_of[i], share[r : r + 1, :], 0.0)
+                for r, spot in enumerate(spots)
+            )
+            high = weight.astype(kind)
+            store(i, high, (weight - high.astype(wide)).astype(kind))
+
+    def keep_weight(i, high, low):
         weights[0, i * capacity : (i + 1) * capacity, :] = high
         weights[1, i * capacity : (i + 1) * capacity, :] = low
+
+    note[...] = jnp.zeros_like(note)
+    note[:TOP, :tok_rows] = logits_ref[...]
+    for j in range(1, pairs):
+        tell(j).start()
+    weigh(spots, share_of(logits_ref[...]), range(ep_count), keep_weight)
     if units < offset:
         both[units:offset, :] = jnp.zeros((offset - units, width), kind)
         both[offset + units :, :] = jnp.zeros((offset - units, width), kind)
@@ -368,7 +434,7 @@
                 beside(i, j).wait_recv()
 
     def raise_hidden(group):
-        result = product(gathered(piece, group), both[...], 1, 1)
+        result = product(gathered(piece, group), turned[...], 1, 0)
         left, right = result[:, :units], result[:, offset : offset + units]
         return (left * jax.nn.sigmoid(left) * right).astype(kind)
 
@@ -415,30 +481,76 @@
         for j in range(1, pairs):
             back_across(i, j).wait_recv()
             total = total + (ymix[j] if i == extra else ybuf[j, i]).astype(wide)
-        total = total.astype(kind)
         if i == extra:
-            mixed_ref[...] = total
-        elif i == 0:
-            returned[0] = total
+            mixed_ref[...] = total.astype(kind)
+        else:
+            abuf[i] = total.astype(kind)
+            home(i).start()
+
+    def settle_near(i):
+        for j in range(1, pairs):
+            back_beside(i, j).wait_recv()
+            block = toward(j) * 2 + side
+            total = (parts[i, block].astype(wide) + cbuf[j, i].astype(wide)).astype(kind)
+            if i == 0:
+                guest_returned[j, near.index(0)] = total
+            else:
+                guest_abuf[j, near.index(i)] = total
+                home_guest(i, j).start()
+        back_beside(i, 0).wait_recv()
+        total = (parts[i, tp].astype(wide) + cbuf[0, i].astype(wide)).astype(kind)
+        if i == 0:
+            returned[i] = total
         else:
             abuf[i] = total
             home(i).start()
 
-    def combine(group):
+    def combine(ref, group, scale):
         start, stop = group[0] * capacity, (group[-1] + 1) * capacity
-        taken = gathered(returned, group)
-        return product(weights[0, start:stop], taken, 0, 0) + product(
-            weights[1, start:stop], taken, 0, 0
+        taken = gathered(ref, group)
+        return product(scale[0, start:stop], taken, 0, 0) + product(
+            scale[1, start:stop], taken, 0, 0
         )
 
-    spare = len(second)
-    quarter = max(1, spare // 4)
-    chunks = [second[n : n + quarter] for n in range(0, spare, quarter)]
+    def expert(group):
+        arrive(group)
+        lower_hidden(group, raise_hidden(group))
+        hand_over(group)
 
     def advance(group):
         for i in group:
             forward(i)
             relay(i - 1)
+
+    def far(group):
+        return [i for i in leaving(group) if i in distant]
+
+    def close(group):
+        return [i for i in leaving(group) if i in near]
+
+    def fold_all(group):
+        for i in group:
+            fold(i)
+
+    def settle_all(group):
+        for i in group:
+            settle(i)
+
+    def settle_close(group):
+        for i in close(group):
+            settle_near(i)
+
+    def keep_guest_weight(i, high, low):
+        at = near.index(i) * capacity
+        guest_weights[0, at : at + capacity, :] = high
+        guest_weights[1, at : at + capacity, :] = low
+
+    bands = [slice(n, n + 128) for n in range(0, 2 * offset, 128)]
+    third_part = -(-len(bands) // 3)
+
+    def turn(part):
+        for band in bands[part * third_part : (part + 1) * third_part]:
+            turned[:, band] = both[band, :].T
 
     recur(0)
     advance(first[1:2])
@@ -447,31 +559,40 @@
     before[...] = jnp.zeros_like(before)
     before_total[...] = jnp.zeros_like(before_total)
     send_window(0)
-    advance(first[2:])
-    advance(chunks[0])
+    for copy in fetch[:2]:
+        copy.wait()
+    turn(0)
+    advance(first[2:3])
+    turn(1)
+    advance(first[3:])
+    turn(2)
+    advance(second[:1])
     arrive(first)
-    for copy in fetch[:3]:
-        copy.wait()
+    fetch[2].wait()
     hidden = raise_hidden(first)
-    for chunk in chunks[1:2]:
-        advance(chunk)
+    advance(second[1:2])
+    lower_hidden(first, hidden)
+    hand_over(far(first) + close(first))
+    advance(second[2:])
+    fold_all(far(first)[-1:])
+    settle_close(first)
     scan()
-    lower_hidden(first, hidden)
-    hand_over(leaving(first))
-    for chunk in chunks[2:]:
-        advance(chunk)
-    for i in leaving(first):
-        fold(i)
-    relay(ep_count - 1)
-    scan()
+    advance(third)
+    fold_all(far(first)[:-1])
     arrive(second)
     hidden = raise_hidden(second)
     lower_hidden(second, hidden)
-    hand_over(leaving(second))
-    for i in leaving(first)[:2]:
-        settle(i)
-    for i in leaving(second):
-        fold(i)
+    hand_over(far(second) + close(second))
+    settle_all(far(first)[-1:])
+    fold_all(far(second))
+    relay(ep_count - 1)
+    scan()
+    settle_all(far(first)[:-1])
+    expert(third)
+    settle_close(second)
+    fold_all(far(third))
+    settle_close(third)
+    settle_all(far(second))
     for _ in range(steps):
         scan()
     for head in range(heads):
@@ -491,32 +612,52 @@
         result = product(lifted_ref[...], matrix[:, cut], 1, 0).astype(kind)
         mix[:, :, cut] = result.reshape(tp_count, mix_rows, stride)
     hand_over([extra])
-    for i in leaving(first)[2:]:
-        settle(i)
     fold(extra)
-    for i in leaving(second):
-        settle(i)
-    for i in first[1:]:
+    for j in range(1, pairs):
+        tell(j).wait_recv()
+        weigh(
+            spots_of(toward(j) * 2 + side),
+            share_of(notes[pairs - j][:TOP, :tok_rows]),
+            near,
+            keep_guest_weight,
+        )
+        for i in near:
+            if i:
+                home_guest(i, j).wait_recv()
+        crossing[j] = combine(guest_returned.at[j], range(len(near)), guest_weights).astype(kind)
+        cross(j).start()
+    settle_all(far(third))
+    for i in first[1:] + second:
         home(i).wait_recv()
-    total = combine(first)
-    for i in second:
+    total = combine(returned, first + second, weights)
+    settle(extra)
+    for i in third:
         home(i).wait_recv()
-    moe_ref[...] = (total + combine(second)).astype(kind)
-    settle(extra)
+    total = total + combine(returned, third, weights)
+    for j in range(1, pairs):
+        cross(j).wait_recv()
+        total = total + crossed[j].astype(wide)
+    moe_ref[...] = total.astype(kind)
 
     for i in range(ep_count):
         if i:
             exchange(i).wait_send()
             home(i).wait_send()
+    for j in range(1, pairs):
+        tell(j).wait_send()
+        cross(j).wait_send()
+        for i in near:
+            if i:
+                home_guest(i, j).wait_send()
+        for i in distant + [extra]:
+            back_across(i, j).wait_send()
+        for i in range(ep_count):
+            across(i, j).wait_send()
     for i in range(ep_count + 1):
         for j in range(pairs):
             back_beside(i, j).wait_send()
-            if j:
-                back_across(i, j).wait_send()
             if i < ep_count:
                 beside(i, j).wait_send()
-                if j:
-                    across(i, j).wait_send()
     for step in range(steps):
 
         @pl.when(me + 2**step < ep_count)
@@ -541,6 +682,7 @@
     mix_rows = seq_len // tp_count
     chunks = (ep_count, capacity, width)
     many = (pairs, ep_count + 1)
+    nearby = (ep_count // 2, capacity, width)
     state = (steps, heads, value_width + 16, key_width)
     return pl.pallas_call(
         functools.partial(kernel, ep_count, tp_count),
@@ -554,9 +696,13 @@
             pltpu.VMEM(chunks, kind),
             pltpu.VMEM((ep_count, tp_count, capacity, width), kind),
             pltpu.VMEM((2 * padded, width), kind),
+            pltpu.VMEM((width, 2 * padded), kind),
             pltpu.VMEM(down.shape, kind),
             pltpu.VMEM(matrix.shape, kind),
             pltpu.VMEM((2, ep_count * capacity, tok_rows), kind),
+            pltpu.VMEM((8, 128), wide),
+            pltpu.VMEM((pairs, 8, 128), wide),
+            pltpu.VMEM((2, nearby[0] * capacity, tok_rows), kind),
             pltpu.VMEM((seq_len, keys), kind),
             pltpu.VMEM((seq_len, values), wide),
             pltpu.VMEM((heads, value_width, key_width), wide),
@@ -575,6 +721,10 @@
             pltpu.VMEM((pairs, mix_rows, width), kind),
             pltpu.VMEM(chunks, kind),
             pltpu.VMEM(chunks, kind),
+            pltpu.VMEM((pairs,) + nearby, kind),
+            pltpu.VMEM((pairs,) + nearby, kind),
+            pltpu.VMEM((pairs, tok_rows, width), kind),
+            pltpu.VMEM((pairs, tok_rows, width), kind),
             dma((4,)),
             dma((ep_count,)),
             dma((ep_count,)),
@@ -590,11 +740,32 @@
             dma(many),
             dma((ep_count,)),
             dma((ep_count,)),
+            dma(many),
+            dma(many),
+            dma((pairs,)),
+            dma((pairs,)),
+            dma((pairs,)),
+            dma((pairs,)),
         ],
         compiler_params=pltpu.CompilerParams(
             collective_id=0, has_side_effects=True, vmem_limit_bytes=60 << 20
         ),
     )(*small, *large)
+
+
+def hand_out_kernel(mixed_in, moe_in, mixed_out, moe_out):
+    mixed_out[...] = mixed_in[...]
+    moe_out[...] = moe_in[...]
+
+
+def hand_out(mixed, moe):
+    vmem = pl.BlockSpec(memory_space=pltpu.VMEM)
+    return pl.pallas_call(
+        hand_out_kernel,
+        out_shape=tuple(jax.ShapeDtypeStruct(part.shape, part.dtype) for part in (mixed, moe)),
+        in_specs=[vmem] * 2,
+        out_specs=(vmem, vmem),
+    )(mixed, moe)
 
 
 def per_device(
@@ -637,7 +808,8 @@
         expert_down_matrix[0],
         recurrence_output_matrix,
     )
-    return run(small, large, surge_log_decay.shape[0], capacity, expert_count, tp_count)
+    heads = surge_log_decay.shape[0]
+    return hand_out(*run(small, large, heads, capacity, expert_count, tp_count))
 
 
 def solution(mesh):

time: 74.6 us -> 68.3 us (0.916); the launches traced: 73.3 us -> 68.2 us
  local copies, waits for them, and re-layouts: 3.34 us -> 0 us
  Pallas kernels: 69.3 us -> 67.5 us
    pallas_call x1, Pallas kernels: 69.3 us -> 65.7 us  [run(): pl.pallas_call(functools.partial(kernel, ep_count, tp_count), out_shape=(...]
    unnamed x2 -> x0, local copies, waits for them, and re-layouts: 3.34 us -> none
    pallas_call x0 -> x1, Pallas kernels: none -> 1.84 us  [hand_out(): pl.pallas_call(hand_out_kernel, out_shape=tuple((jax.ShapeDtypeStruct(par...]
where the time goes in v2:
time: 68.3 us; the launch traced here: 68.2 us
  Pallas kernels  67.5 us (99%)
    pallas_call x1, Pallas kernels, run(): pl.pallas_call(functools.partial(kernel, ep_count, tp_count), out_shape=(...  65.7 us
    pallas_call x1, Pallas kernels, hand_out(): pl.pallas_call(hand_out_kernel, out_shape=tuple((jax.ShapeDtypeStruct(par...  1.84 us

profile of v2, /device:TPU:0, one launch (start us, length us, event | category | flops | bytes accessed | tf_op | source)
XLA Modules:
  0.0 68.2 jit_solution(16107427276781719045)
XLA Ops:
  0.6 65.7 %shard_map.158 = (bf16[32,4096]{1,0:T(8,128)(2,1)}, bf16[32,4096]{1,0:T(8,128)(2,1)}) custom-call(bf16[128,256]{1,0:T(8,128)(2,1)} %query_ref.1, bf16[128,256]{1,0:T(8,128)(2,1)} %forget_ref.1, bf16[128,256]{1,0:T(8,128)(2,1)} %value_ref.1, bf16[128,256]{1,0:T(8,128)(2,1)} %opening_ref.1, f32[1,256]{1,0:T(1,128)} %bitcast.16, f32[2,128]{1,0:T(2,128)} %surge_ref.1, ...), custom_call_target="tpu_custom_call" | custom-call | tf_op jit(solution)/shard_map/pallas_call | solution.py:687
  66.3 1.8 %shard_map.159 = (bf16[32,4096]{1,0:T(8,128)(2,1)}, bf16[32,4096]{1,0:T(8,128)(2,1)}) custom-call(bf16[32,4096]{1,0:T(8,128)(2,1)} %get-tuple-element.4.mixed_in, bf16[32,4096]{1,0:T(8,128)(2,1)} %get-tuple-element.5.moe_in), custom_call_target="tpu_custom_call" | custom-call | tf_op jit(solution)/shard_map/pallas_call | solution.py:763

commit v3 on v2

--- a/solution.py
+++ b/solution.py
@@ -79,6 +79,7 @@
 def kernel(
     ep_count,
     tp_count,
+    pending,
     query_ref,
     forget_ref,
     value_ref,
@@ -172,7 +173,6 @@
     whole_tiles = capacity % 16 == 0
     stride = min(width, 1024) if whole_tiles else width
 
-    greet(me, tp, ep_count, tp_count)
     fetch = [
         pltpu.make_async_copy(gate_hbm, both.at[pl.ds(0, units)], load.at[0]),
         pltpu.make_async_copy(up_hbm, both.at[pl.ds(offset, units)], load.at[1]),
@@ -344,6 +344,8 @@
         both[units:offset, :] = jnp.zeros((offset - units, width), kind)
         both[offset + units :, :] = jnp.zeros((offset - units, width), kind)
 
+    for copy in pending:
+        copy.wait()
     at, since = iota((seq_len, seq_len), 0), iota((seq_len, seq_len), 1)
     shut = jax.nn.sigmoid(-forget_ref[...].astype(wide)) * margin_ref[...]
     within = ((at >= since) & (at // SPAN == since // SPAN)).astype(wide)
@@ -566,6 +568,14 @@
     turn(1)
     advance(first[3:])
     turn(2)
+    for j in range(1, pairs):
+        tell(j).wait_recv()
+        weigh(
+            spots_of(toward(j) * 2 + side),
+            share_of(notes[pairs - j][:TOP, :tok_rows]),
+            near,
+            keep_guest_weight,
+        )
     advance(second[:1])
     arrive(first)
     fetch[2].wait()
@@ -614,13 +624,6 @@
     hand_over([extra])
     fold(extra)
     for j in range(1, pairs):
-        tell(j).wait_recv()
-        weigh(
-            spots_of(toward(j) * 2 + side),
-            share_of(notes[pairs - j][:TOP, :tok_rows]),
-            near,
-            keep_guest_weight,
-        )
         for i in near:
             if i:
                 home_guest(i, j).wait_recv()
@@ -665,11 +668,27 @@
             state_copy(step).wait_send()
 
 
+def entry(ep_count, tp_count, count, *refs):
+    greet(lax.axis_index("ep"), lax.axis_index("tp"), ep_count, tp_count)
+    sources, rest = refs[:count], refs[count:]
+    middle, staged, arrived, rest = rest[:6], rest[6 : 6 + count], rest[6 + count], rest[7 + count :]
+    copies = [
+        pltpu.make_async_copy(source, stage, arrived.at[n])
+        for n, (source, stage) in enumerate(zip(sources, staged))
+    ]
+    for copy in copies[7:] + copies[:7]:
+        copy.start()
+    for copy in copies[7:]:
+        copy.wait()
+    kernel(ep_count, tp_count, copies[:7], *staged, *middle, *rest)
+
+
 def run(small, large, heads, capacity, ep_count, tp_count):
     pairs = tp_count // 2
     dma = pltpu.SemaphoreType.DMA
     vmem = pl.BlockSpec(memory_space=pltpu.VMEM)
     hbm = pl.BlockSpec(memory_space=pl.ANY)
+    far = pl.BlockSpec(memory_space=pltpu.HBM)
     query, value, tokens = small[0], small[2], small[7]
     gate, _, down, matrix = large
     seq_len, keys = query.shape
@@ -685,14 +704,16 @@
     nearby = (ep_count // 2, capacity, width)
     state = (steps, heads, value_width + 16, key_width)
     return pl.pallas_call(
-        functools.partial(kernel, ep_count, tp_count),
+        functools.partial(entry, ep_count, tp_count, len(small)),
         out_shape=(
             jax.ShapeDtypeStruct((mix_rows, width), kind),
             jax.ShapeDtypeStruct((tok_rows, width), kind),
         ),
-        in_specs=[vmem] * len(small) + [hbm] * len(large),
+        in_specs=[far] * len(small) + [hbm] * len(large),
         out_specs=(vmem, vmem),
-        scratch_shapes=[
+        scratch_shapes=[pltpu.VMEM(part.shape, part.dtype) for part in small]
+        + [
+            dma((len(small),)),
             pltpu.VMEM(chunks, kind),
             pltpu.VMEM((ep_count, tp_count, capacity, width), kind),
             pltpu.VMEM((2 * padded, width), kind),

time: 68.3 us -> 68 us (level)
  Pallas kernels: 67.5 us -> 66.6 us
    pallas_call x1, Pallas kernels: 65.7 us -> 64.8 us  [run(): pl.pallas_call(functools.partial(entry, ep_count, tp_count, len(small)),...]
where the time goes in v3:
time: 68 us; the launch traced here: 67.3 us
  Pallas kernels  66.6 us (98%)
    pallas_call x1, Pallas kernels, run(): pl.pallas_call(functools.partial(entry, ep_count, tp_count, len(small)),...  64.8 us
    pallas_call x1, Pallas kernels, hand_out(): pl.pallas_call(hand_out_kernel, out_shape=tuple((jax.ShapeDtypeStruct(par...  1.84 us

profile of v3, /device:TPU:0, one launch (start us, length us, event | category | flops | bytes accessed | tf_op | source)
XLA Modules:
  0.0 67.3 jit_solution(1097089090471677232)
XLA Ops:
  0.6 64.8 %shard_map.158 = (bf16[32,4096]{1,0:T(8,128)(2,1)}, bf16[32,4096]{1,0:T(8,128)(2,1)}) custom-call(bf16[128,256]{1,0:T(8,128)(2,1)} %refs_0_.1, bf16[128,256]{1,0:T(8,128)(2,1)} %refs_1_.1, bf16[128,256]{1,0:T(8,128)(2,1)} %refs_2_.1, bf16[128,256]{1,0:T(8,128)(2,1)} %refs_3_.1, f32[1,256]{1,0:T(1,128)} %bitcast.16, f32[2,128]{1,0:T(2,128)} %refs_5_.1, ...), custom_call_target="tpu_custom_call" | custom-call | tf_op jit(solution)/shard_map/pallas_call | solution.py:706
  65.5 1.8 %shard_map.159 = (bf16[32,4096]{1,0:T(8,128)(2,1)}, bf16[32,4096]{1,0:T(8,128)(2,1)}) custom-call(bf16[32,4096]{1,0:T(8,128)(2,1)} %get-tuple-element.4.mixed_in, bf16[32,4096]{1,0:T(8,128)(2,1)} %get-tuple-element.5.moe_in), custom_call_target="tpu_custom_call" | custom-call | tf_op jit(solution)/shard_map/pallas_call | solution.py:784
